TPU v7x, 512 devices: a whole 4x8x8 slice. The times are simulated.
512 devices in a mesh: sp: 32 (over z, x), tp: 16 (over y, core).
Axes of the slice: x: 4, y: 8, z: 8, core: 2. Of those that a mesh axis runs over, the one named last changes fastest.
Arguments:
- resid: bfloat16 [16384, 2048], P(('sp', 'tp')), may hold values from -6 to 6
- recurrent_input: bfloat16 [16384, 2048], P('sp', 'tp'), may hold values from -12.2 to 12.2
- recurrent_out_gate: bfloat16 [16384, 2048], P('sp', 'tp'), may hold values from -6 to 6
- filter_weight: float32 [4, 2048], P(None, 'tp'), may hold values from -3 to 3
- recurrence_gate_matrix: bfloat16 [32, 64, 64], P('tp'), may hold values from -0.75 to 0.75
- input_gate_matrix: bfloat16 [32, 64, 64], P('tp'), may hold values from -0.75 to 0.75
- channel_decay_raw: float32 [2048], P('tp'), may hold values from 4.8 to 13.5
- token_decay_boost: float32 [16384, 2048], P('sp', 'tp'), may hold values from -0.7 to 0
- output_projection_weight: bfloat16 [2048, 2048], P('tp'), may hold values from -0.375 to 0.375
- expert_norm_gain: float32 [2048], replicated, may hold values from 0.1 to 1.9
- routes: int32 [16384, 2], P('sp'), may hold values from 0 to 31, all different within a row; in each aligned block of 32 rows (0 to 31, 32 to 63, ...) at most 3 rows name the same one
- expert_pair_weight: float32 [16384, 2], P(('sp', 'tp')), may hold values from 0.2 to 0.8
- gate_weight: bfloat16 [32, 2048, 2048], P('sp', None, 'tp'), may hold values from -0.125 to 0.125
- up_weight: bfloat16 [32, 2048, 2048], P('sp', None, 'tp'), may hold values from -0.125 to 0.125
- down_weight: bfloat16 [32, 2048, 2048], P('sp', None, 'tp'), may hold values from -0.25 to 0.25
Outputs:
- layer_out: bfloat16 [16384, 2048], P(('sp', 'tp'))
Inputs may be any that keep to these rules, and one draw needn't show every extreme that they name: `routes`: in each aligned block of 32 rows no expert is named by more than 3 rows, and the two experts of a row differ.
All inputs are finite; a program needn't handle non-finite values.
Results may differ from a plain program's by a relative error of at most 0.013.
Values may be sent and summed in bfloat16 or wider, within the bound.
No kernel may reach another device: no remote copies, remote signals or barrier semaphores. Data moves between devices by JAX's collectives and lax.ppermute only.
A program may use at most 64 MiB of HBM per device.

v0:
```python
import jax
import jax.numpy as jnp
from jax import lax
from jax.sharding import PartitionSpec as P

RECURRENT_SCALE = 8.0
EPSILON = 1e-06


def shifted(block, axis, distance):
    devices = range(lax.axis_size(axis))
    route = [(i - distance, i) for i in devices if i - distance in devices]
    return lax.ppermute(block, axis, route)


def from_everyone(x, axis):
    size = lax.axis_size(axis)
    return lax.all_to_all(jnp.broadcast_to(x[None], (size, *x.shape)), axis, 0, 0, tiled=True)


def collected_together(x, axis):
    leaves = jax.tree.leaves(x)
    order = sorted(range(len(leaves)), key=lambda k: -leaves[k].size)
    width = (1, *leaves[order[0]].shape)[-1]
    lines = [
        jnp.pad(leaves[k].reshape(-1), (0, -leaves[k].size % width)).reshape(-1, width)
        for k in order
    ]
    both, at, found = (from_everyone(jnp.concatenate(lines), axis), 0, {})
    for k, line in zip(order, lines):
        slab = both[:, at : at + len(line)].reshape(len(both), -1)
        found[k] = slab[:, : leaves[k].size].reshape(-1, *leaves[k].shape)
        at += len(line)
    numbers = iter(range(len(leaves)))
    return jax.tree.map(lambda _: found[next(numbers)], x)


def joined_by_halves(pieces, combine):
    while len(jax.tree.leaves(pieces)[0]) > 1:
        pieces = jax.vmap(combine)(
            *(jax.tree.map(lambda part: part[side::2], pieces) for side in (0, 1))
        )
    return jax.tree.map(lambda part: part[0], pieces)


def carried_in(x, axis, combine, identity):
    size, position = (lax.axis_size(axis), lax.axis_index(axis))
    passed = jnp.arange(size) < position

    def kept(part, zero, own):
        part = jnp.where(
            passed.reshape(-1, *(1 for _ in own.shape)), part, jnp.asarray(zero, own.dtype)
        )
        return part

    pieces = collected_together(x, axis)
    return joined_by_halves(jax.tree.map(kept, pieces, identity, x), combine)


def split_up(x, dim, size):
    before, after = (x.shape[:dim], x.shape[dim + 1 :])
    return jnp.moveaxis(x.reshape(*before, size, -1, *after), dim, 0)


def sum_at_owner(x, axis, dim):
    pieces = split_up(x, dim, lax.axis_size(axis))
    arrived = lax.all_to_all(pieces, axis, split_axis=0, concat_axis=0, tiled=True)
    return arrived.astype(jnp.float32).sum(axis=0)


def in_order(pieces, dim):
    pieces = jnp.moveaxis(pieces, 0, dim)
    dims = pieces.shape
    return pieces.reshape(*dims[:dim], dims[dim] * dims[dim + 1], *dims[dim + 2 :])


def piecewise(x, axis, dim, work, out_dim):
    extent = x.shape[dim]
    pieces = jnp.split(x, 2, axis=dim) if extent % 2 == 0 else [x]
    first = jnp.arange(lax.axis_size(axis)) * extent
    blocks = [lax.all_gather(slab, axis) for slab in pieces]
    made = [jax.vmap(work)(b, first + k * (extent // len(pieces))) for k, b in enumerate(blocks)]
    return in_order(jnp.concatenate(made, axis=out_dim + 1), out_dim)


def chain_step(earlier, later):
    return (earlier[0] * later[0], later[0] * earlier[1] + later[1])


def slot_numbers(picks, experts):
    flat = picks.reshape(-1)
    onehot = (flat[:, None] == jnp.arange(experts, dtype=jnp.int32)[None, :]).astype(jnp.int32)
    before = jnp.cumsum(onehot, axis=0) - onehot
    return (flat, jnp.sum(before * onehot, axis=1))


def fill_slots(source_rows, slot_of, row_of, slot_count):
    match = slot_of[None, :] == jnp.arange(slot_count, dtype=jnp.int32)[:, None]
    picked = jnp.sum(jnp.where(match, row_of[None, :], 0), axis=1)
    present = jnp.any(match, axis=1)
    return jnp.where(present[:, None], source_rows[picked], jnp.zeros((), source_rows.dtype))


def expert_hidden(rows, gate_weight, up_weight):
    gate = jnp.dot(rows, gate_weight[0], preferred_element_type=jnp.float32)
    upward = jnp.dot(rows, up_weight[0], preferred_element_type=jnp.float32)
    return (jax.nn.silu(gate) * upward).astype(jnp.bfloat16)


def expert_down(active, down_weight):
    columns = down_weight[0]
    return jnp.dot(
        lax.all_gather(active, "tp", axis=1, tiled=True),
        columns,
        preferred_element_type=jnp.float32,
    ).astype(jnp.bfloat16)


def body(
    resid,
    recurrent_input,
    recurrent_out_gate,
    filter_weight,
    recurrence_gate_matrix,
    input_gate_matrix,
    channel_decay_raw,
    token_decay_boost,
    output_projection_weight,
    expert_norm_gain,
    routes,
    expert_pair_weight,
    gate_weight,
    up_weight,
    down_weight,
):
    tokens_here, channels = recurrent_input.shape
    taps = filter_weight.shape[0]
    rim = shifted(recurrent_input[tokens_here - taps + 1 :], "sp", 1)
    extended = jnp.concatenate([rim, recurrent_input], axis=0).astype(jnp.float32)
    mixed_in = extended[0:tokens_here] * filter_weight[0]
    for offset in range(1, taps):
        mixed_in = mixed_in + extended[offset : offset + tokens_here] * filter_weight[offset]
    smoothed = mixed_in.astype(jnp.bfloat16)
    grouped = smoothed.reshape(
        tokens_here, recurrence_gate_matrix.shape[0], recurrence_gate_matrix.shape[1]
    )
    recurrence_gate = jax.nn.sigmoid(
        jnp.einsum(
            "tni,nij->tnj", grouped, recurrence_gate_matrix, preferred_element_type=jnp.float32
        ).reshape(tokens_here, channels)
    )
    input_gate = jax.nn.sigmoid(
        jnp.einsum(
            "tni,nij->tnj", grouped, input_gate_matrix, preferred_element_type=jnp.float32
        ).reshape(tokens_here, channels)
    )
    decay_logarithm = (
        -RECURRENT_SCALE * recurrence_gate * jax.nn.softplus(-channel_decay_raw) + token_decay_boost
    )
    decay = jnp.exp(decay_logarithm)
    drive = jnp.sqrt(-jnp.expm1(2.0 * decay_logarithm)) * (
        input_gate * smoothed.astype(jnp.float32)
    )
    running, local_state = lax.associative_scan(chain_step, (decay, drive), axis=0)
    identity = (jnp.ones((channels,), jnp.float32), jnp.zeros((channels,), jnp.float32))
    carried = carried_in((running[-1], local_state[-1]), "sp", chain_step, identity)
    state = local_state + running * carried[1][None, :]
    branch = (jax.nn.gelu(recurrent_out_gate.astype(jnp.float32)) * state).astype(jnp.bfloat16)
    tp_size = lax.axis_size("tp")
    rows_dev = tokens_here // tp_size
    projected = sum_at_owner(
        jnp.dot(branch, output_projection_weight, preferred_element_type=jnp.float32).astype(
            jnp.bfloat16
        ),
        "tp",
        0,
    )
    stream = (resid.astype(jnp.float32) + projected).astype(jnp.bfloat16)
    stream_wide = stream.astype(jnp.float32)
    normed = (
        stream_wide
        * lax.rsqrt(jnp.mean(stream_wide * stream_wide, axis=1, keepdims=True) + EPSILON)
        * expert_norm_gain
    ).astype(jnp.bfloat16)
    model_width = normed.shape[1]
    experts = lax.axis_size("sp")
    capacity = max(2, 3 * rows_dev // experts)
    own_routes = lax.dynamic_slice_in_dim(routes, lax.axis_index("tp") * rows_dev, rows_dev, 0)
    own_flat, own_rank = slot_numbers(own_routes, experts)
    own_slots = own_flat * capacity + own_rank
    row_of = jnp.arange(2 * rows_dev, dtype=jnp.int32) // 2
    outgoing = fill_slots(normed, own_slots, row_of, experts * capacity).reshape(
        experts, capacity, model_width
    )
    arrived = lax.all_to_all(outgoing, "sp", split_axis=0, concat_axis=0, tiled=True)

    def hidden_piece(piece, start):
        flat_rows = piece.reshape(piece.shape[0] * piece.shape[1], model_width)
        return expert_hidden(flat_rows, gate_weight, up_weight).reshape(
            piece.shape[0], piece.shape[1], -1
        )

    active = piecewise(
        arrived.reshape(1, experts * capacity, model_width), "tp", 0, hidden_piece, 0
    )
    result = expert_down(active.reshape(-1, active.shape[2]), down_weight)
    joined = lax.all_to_all(
        result.reshape(tp_size, experts * capacity, -1),
        "tp",
        split_axis=0,
        concat_axis=2,
        tiled=True,
    )
    returned = lax.all_to_all(
        joined.reshape(experts, capacity, model_width),
        "sp",
        split_axis=0,
        concat_axis=0,
        tiled=True,
    )
    picked = (
        returned.reshape(experts * capacity, model_width)[own_slots]
        .astype(jnp.float32)
        .reshape(rows_dev, 2, model_width)
    )
    blended = jnp.sum(picked * expert_pair_weight[:, :, None], axis=1)
    return (stream_wide + blended).astype(jnp.bfloat16)


def solution(mesh):
    placed = (
        P(("sp", "tp"), None),
        P("sp", "tp"),
        P("sp", "tp"),
        P(None, "tp"),
        P("tp", None, None),
        P("tp", None, None),
        P("tp"),
        P("sp", "tp"),
        P("tp", None),
        P(),
        P("sp", None),
        P(("sp", "tp"), None),
        P("sp", None, "tp"),
        P("sp", None, "tp"),
        P("sp", None, "tp"),
    )
    return jax.shard_map(
        body, mesh=mesh, in_specs=placed, out_specs=P(("sp", "tp"), None), check_vma=False
    )
```

profile of v0, /device:TPU:1, one launch (start us, length us, event | category | flops | bytes accessed | tf_op | source)
XLA Modules:
  0.0 395.7 jit_solution(9061123407506774359)
XLA Ops:
  7.4 3.9 collective-permute-start
  19.0 4.5 %slice.371 = f32[256,128]{0,1:T(8,128)S(1)} slice(f32[512,128]{0,1:T(8,128)S(1)} %get-tuple-element.9), slice={[0:511:2], [0:128:1]} | slice | bytes 262144 | tf_op jit(solution)/shard_map/slice | solution.py:164
  23.5 4.5 %slice.372 = f32[256,128]{0,1:T(8,128)S(1)} slice(f32[512,128]{0,1:T(8,128)S(1)} %get-tuple-element.9), slice={[1:512:2], [0:128:1]} | slice | bytes 262144 | tf_op jit(solution)/shard_map/slice | solution.py:164
  27.9 4.5 %slice.370 = f32[256,128]{0,1:T(8,128)S(1)} slice(f32[512,128]{0,1:T(8,128)S(1)} %get-tuple-element.10), slice={[1:512:2], [0:128:1]} | slice | bytes 262144 | tf_op jit(solution)/shard_map/slice | solution.py:164
  32.4 5.0 %slice.374 = f32[256,128]{0,1:T(8,128)S(1)} slice(f32[512,128]{0,1:T(8,128)S(1)} %get-tuple-element.10), slice={[0:511:2], [0:128:1]} | slice | bytes 262144 | tf_op jit(solution)/shard_map/slice | solution.py:164
  67.1 4.5 %slice.369 = f32[255,128]{0,1:T(8,128)S(1)} slice(f32[512,128]{0,1:T(8,128)S(1)} %get-tuple-element.10), slice={[2:512:2], [0:128:1]} | slice | bytes 261120 | tf_op jit(solution)/shard_map/slice | solution.py:164
  71.5 4.9 %slice.434 = f32[255,128]{0,1:T(8,128)S(1)} slice(f32[512,128]{0,1:T(8,128)S(1)} %get-tuple-element.9), slice={[2:512:2], [0:128:1]} | slice | bytes 261120 | tf_op jit(solution)/shard_map/slice | solution.py:164
  94.1 4.5 %pad.145 = f32[512,128]{0,1:T(8,128)S(1)} pad(f32[256,128]{0,1:T(8,128)S(1)} %add.346, f32[]{:T(128)} %constant.25.clone.1), padding=1_0_1x0_0_0 | pad | bytes 393220 | tf_op jit(solution)/shard_map/pad | solution.py:164
  103.3 4.4 %pad.144 = f32[512,128]{0,1:T(8,128)S(1)} pad(f32[256,128]{0,1:T(8,128)S(1)} %pad_maximum_fusion.1, f32[]{:T(128)} %constant.25.clone.1), padding=0_1_1x0_0_0 | pad | bytes 393220 | tf_op jit(solution)/shard_map/pad | solution.py:164
  107.9 4.6 %pad.127 = f32[512,128]{0,1:T(8,128)S(1)} pad(f32[256,128]{0,1:T(8,128)S(1)} %add.336, f32[]{:T(128)} %constant.25.clone.1), padding=1_0_1x0_0_0 | pad | bytes 393220 | tf_op jit(solution)/shard_map/pad | solution.py:164
  112.6 4.4 %pad.126 = f32[512,128]{0,1:T(8,128)S(1)} pad(f32[256,128]{0,1:T(8,128)S(1)} %pad_maximum_fusion, f32[]{:T(128)} %constant.25.clone.1), padding=0_1_1x0_0_0 | pad | bytes 393220 | tf_op jit(solution)/shard_map/pad | solution.py:164
  117.8 12.6 %all-to-all-start = ((f32[32,2,128]{2,1,0:T(2,128)}), f32[32,2,128]{2,1,0:T(2,128)S(1)}, u32[]{:S(2)}, u32[]{:S(2)}) async-start(f32[32,2,128]{2,1,0:T(2,128)} %broadcast_in_dim.64), calls=%async_computation | async-start | bytes 65536 | tf_op jit(solution)/shard_map/all_to_all | solution.py:18
  130.4 8.7 %all-to-all-done = f32[32,2,128]{2,1,0:T(2,128)S(1)} async-done(((f32[32,2,128]{2,1,0:T(2,128)}), f32[32,2,128]{2,1,0:T(2,128)S(1)}, u32[]{:S(2)}, u32[]{:S(2)}) %all-to-all-start) | async-done | bytes 32800 | tf_op jit(solution)/shard_map/all_to_all | solution.py:18
  141.7 9.5 %all-to-all-start.1 = ((bf16[16,32,2048]{2,1,0:T(8,128)(2,1)}), bf16[16,32,2048]{2,1,0:T(8,128)(2,1)S(1)}, u32[]{:S(2)}, u32[]{:S(2)}) async-start(bf16[16,32,2048]{2,1,0:T(8,128)(2,1)} %bitcast.12), calls=%async_computation.1 | async-start | bytes 4194304 | tf_op jit(solution)/shard_map/all_to_all | solution.py:67
  152.9 47.3 %all-to-all-done.1 = bf16[16,32,2048]{2,1,0:T(8,128)(2,1)S(1)} async-done(((bf16[16,32,2048]{2,1,0:T(8,128)(2,1)}), bf16[16,32,2048]{2,1,0:T(8,128)(2,1)S(1)}, u32[]{:S(2)}, u32[]{:S(2)}) %all-to-all-start.1) | async-done | bytes 2097184 | tf_op jit(solution)/shard_map/all_to_all | solution.py:67
  202.3 19.6 %all_to_all.35 = bf16[32,3,2048]{2,1,0:T(4,128)(2,1)S(1)} all-to-all(bf16[32,3,2048]{2,1,0:T(4,128)(2,1)S(1)} %broadcast_select_fusion), channel_id=1, replica_groups=mesh['sp'=32,'tp'=16] {'sp'}, dimensions={0} | all-to-all | bytes 786432 | tf_op jit(solution)/shard_map/all_to_all | solution.py:195
  223.3 43.7 %all-gather.3.cloned.1.call-done = bf16[16,1,96,2048]{3,2,1,0:T(8,128)(2,1)} async-done(((bf16[1,1,96,2048]{3,2,1,0:T(8,128)(2,1)}), bf16[16,1,96,2048]{3,2,1,0:T(8,128)(2,1)}) %all-gather.3.cloned.1.call-update) | async-done | bytes 6291472 | tf_op jit(solution)/shard_map/all_gather | solution.py:81
  267.0 4.7 %fusion.2 = f32[16,96,128]{2,1,0:T(8,128)S(1)} fusion(bf16[16,1,96,2048]{3,2,1,0:T(8,128)(2,1)} %all-gather.3.cloned.1.call-done, bf16[1,2048,128]{2,1,0:T(8,128)(2,1)S(1)} %copy-done.5), kind=kOutput, calls=%fused_computation.4 | convolution fusion | flops 805306368 | bytes 7602176 | tf_op jit(solution)/shard_map/vmap()/dot_general | solution.py:105
  271.7 2.6 fusion.7
  274.4 58.5 %all-gather.5.cloned.1.call-done = bf16[1536,2048]{1,0:T(8,128)(2,1)} async-done(((bf16[1536,128]{1,0:T(8,128)(2,1)}), bf16[1536,2048]{1,0:T(8,128)(2,1)}) %all-gather.5.cloned.1.call-update) | async-done | bytes 6291472 | tf_op jit(solution)/shard_map/all_gather | solution.py:113
  332.9 4.6 %convolution_convert_fusion.1 = bf16[1536,128]{1,0:T(8,128)(2,1)S(1)} fusion(bf16[1536,2048]{1,0:T(8,128)(2,1)} %all-gather.5.cloned.1.call-done, bf16[1,2048,128]{2,1,0:T(8,128)(2,1)S(1)} %copy-done.7), kind=kOutput, calls=%fused_computation.8 | convolution fusion | flops 805502976 | bytes 7208960 | tf_op jit(solution)/shard_map/dot_general | solution.py:112
  337.5 19.4 %all_to_all.36 = bf16[16,96,128]{2,1,0:T(8,128)(2,1)S(1)} all-to-all(bf16[16,96,128]{2,1,0:T(8,128)(2,1)S(1)} %bitcast.97), channel_id=1, replica_groups=mesh['sp'=32,'tp'=16] {'tp'}, dimensions={0} | all-to-all | bytes 786432 | tf_op jit(solution)/shard_map/all_to_all | solution.py:207
  357.9 9.9 %all-to-all-start.4 = ((bf16[32,3,2048]{2,1,0:T(4,128)(2,1)}), bf16[32,3,2048]{2,1,0:T(4,128)(2,1)S(1)}, u32[]{:S(2)}, u32[]{:S(2)}) async-start(bf16[32,3,2048]{2,1,0:T(4,128)(2,1)} %reshape.148), calls=%async_computation.4 | async-start | bytes 1048576 | tf_op jit(solution)/shard_map/all_to_all | solution.py:214
  368.2 17.4 %all-to-all-done.4 = bf16[32,3,2048]{2,1,0:T(4,128)(2,1)S(1)} async-done(((bf16[32,3,2048]{2,1,0:T(4,128)(2,1)}), bf16[32,3,2048]{2,1,0:T(4,128)(2,1)S(1)}, u32[]{:S(2)}, u32[]{:S(2)}) %all-to-all-start.4) | async-done | bytes 393248 | tf_op jit(solution)/shard_map/all_to_all | solution.py:214
  (231 shorter events, 72.6 us)
Async XLA Ops:
  6.5 133.0 %copy-start = (bf16[128,2048]{1,0:T(8,128)(2,1)S(1)}, bf16[128,2048]{1,0:T(8,128)(2,1)}, u32[]{:S(2)}) copy-start(bf16[128,2048]{1,0:T(8,128)(2,1)} %param.23) | copy-start | bytes 1572868
  7.4 8.6 %collective-permute-start = (bf16[3,128]{0,1:T(8,128)(2,1)S(1)}, bf16[3,128]{0,1:T(8,128)(2,1)S(1)}, u32[]{:S(2)}, u32[]{:S(2)}) collective-permute-start(bf16[3,128]{0,1:T(8,128)(2,1)S(1)} %copy.84), channel_id=1, source_target_pairs={{0,16},{16,32},{32,48},{48,64},{64,80},{80,96},{96,112},{112,128},... | collective-permute-start | bytes 2312 | tf_op jit(solution)/shard_map/ppermute | solution.py:13
  107.8 92.8 %copy-start.1 = (bf16[32,2048]{1,0:T(8,128)(2,1)S(1)}, bf16[32,2048]{1,0:T(8,128)(2,1)}, u32[]{:S(2)}) copy-start(bf16[32,2048]{1,0:T(8,128)(2,1)} %param.15) | copy-start | bytes 393220
  112.4 88.3 %copy-start.2 = (f32[2048]{0:T(1024)S(1)}, f32[2048]{0:T(1024)}, u32[]{:S(2)}) copy-start(f32[2048]{0:T(1024)} %param.24) | copy-start | bytes 24580
  117.8 21.3 %all-to-all-start = ((f32[32,2,128]{2,1,0:T(2,128)}), f32[32,2,128]{2,1,0:T(2,128)S(1)}, u32[]{:S(2)}, u32[]{:S(2)}) async-start(f32[32,2,128]{2,1,0:T(2,128)} %broadcast_in_dim.64), calls=%async_computation | async-start | bytes 65536 | tf_op jit(solution)/shard_map/all_to_all | solution.py:18
  141.7 58.5 %all-to-all-start.1 = ((bf16[16,32,2048]{2,1,0:T(8,128)(2,1)}), bf16[16,32,2048]{2,1,0:T(8,128)(2,1)S(1)}, u32[]{:S(2)}, u32[]{:S(2)}) async-start(bf16[16,32,2048]{2,1,0:T(8,128)(2,1)} %bitcast.12), calls=%async_computation.1 | async-start | bytes 4194304 | tf_op jit(solution)/shard_map/all_to_all | solution.py:67
  151.2 115.8 %copy-start.5 = (bf16[1,2048,128]{2,1,0:T(8,128)(2,1)S(1)}, bf16[1,2048,128]{2,1,0:T(8,128)(2,1)}, u32[]{:S(2)}) copy-start(bf16[1,2048,128]{2,1,0:T(8,128)(2,1)} %param.27) | copy-start | bytes 1572868
  151.2 115.8 %all-gather.3.cloned.1.call-start = ((), (), s32[]{:S(2)}) async-start(), calls=%async_computation.5 | async-start | bytes 6684672 | tf_op jit(solution)/shard_map/all_gather | solution.py:81
  223.0 48.8 %copy-start.6 = (bf16[1,2048,128]{2,1,0:T(8,128)(2,1)S(1)}, bf16[1,2048,128]{2,1,0:T(8,128)(2,1)}, u32[]{:S(2)}) copy-start(bf16[1,2048,128]{2,1,0:T(8,128)(2,1)} %param.28) | copy-start | bytes 1572868
  223.0 109.9 %all-gather.5.cloned.1.call-start = ((), (), s32[]{:S(2)}) async-start(), calls=%async_computation.6 | async-start | bytes 6684672 | tf_op jit(solution)/shard_map/all_gather | solution.py:113
  267.0 4.8 %copy-start.4 = (bf16[16,1,96,2048]{3,2,1,0:T(8,128)(2,1)S(1)}, bf16[16,1,96,2048]{3,2,1,0:T(8,128)(2,1)}, u32[]{:S(2)}) copy-start(bf16[16,1,96,2048]{3,2,1,0:T(8,128)(2,1)} %all-gather.3.cloned.1.call-done) | copy-start | bytes 18874372
  271.7 61.1 %copy-start.7 = (bf16[1,2048,128]{2,1,0:T(8,128)(2,1)S(1)}, bf16[1,2048,128]{2,1,0:T(8,128)(2,1)}, u32[]{:S(2)}) copy-start(bf16[1,2048,128]{2,1,0:T(8,128)(2,1)} %param.29) | copy-start | bytes 1572868
  274.3 93.7 %copy-start.3 = (f32[32,2]{0,1:T(2,128)S(1)}, f32[32,2]{0,1:T(2,128)}, u32[]{:S(2)}) copy-start(f32[32,2]{0,1:T(2,128)} %param.26) | copy-start | bytes 772
  357.9 27.6 %all-to-all-start.4 = ((bf16[32,3,2048]{2,1,0:T(4,128)(2,1)}), bf16[32,3,2048]{2,1,0:T(4,128)(2,1)S(1)}, u32[]{:S(2)}, u32[]{:S(2)}) async-start(bf16[32,3,2048]{2,1,0:T(4,128)(2,1)} %reshape.148), calls=%async_computation.4 | async-start | bytes 1048576 | tf_op jit(solution)/shard_map/all_to_all | solution.py:214
Sparse Core Ops, SparseCore 0:
  223.1 43.8 all-gather.2
  274.5 58.3 all-gather.4
where the time goes:
time: 403 us; the launch traced here: 396 us
  waiting for transfers between devices  176 us (44%)
  local copies, waits for them, and re-layouts  105 us (26%)
  blocking collectives  39 us (10%)
  starting transfers between devices  36.2 us (9%)
  matrix products  16.1 us (4%)
  between operations  15.1 us (4%)
  other arithmetic  8.3 us (2%)
    all_gather x1, waiting for transfers between devices, expert_down(): lax.all_gather(active, 'tp', axis=1, tiled=True)  58.5 us
    slice x50, local copies, waits for them, and re-layouts, body(): lax.associative_scan(chain_step, (decay, drive), axis=0)  56 us
    all_to_all x1, waiting for transfers between devices, sum_at_owner(): lax.all_to_all(pieces, axis, split_axis=0, concat_axis=0, tiled=True)  47.3 us
    all_gather x1, waiting for transfers between devices, piecewise(): blocks = [lax.all_gather(slab, axis) for slab in pieces]  43.7 us
    pad x32, local copies, waits for them, and re-layouts, body(): lax.associative_scan(chain_step, (decay, drive), axis=0)  36.4 us
    all_to_all x1, blocking collectives, body(): lax.all_to_all(outgoing, 'sp', split_axis=0, concat_axis=0, tiled=True)  19.6 us
    all_to_all x1, blocking collectives, body(): lax.all_to_all(result.reshape(tp_size, experts * capacity, -1), 'tp', spl...  19.4 us
    all_to_all x1, waiting for transfers between devices, body(): lax.all_to_all(joined.reshape(experts, capacity, model_width), 'sp', spli...  17.4 us
  transfers between devices with their start and end apart: 6, of which 5 were waited for; matrix products, arithmetic and copies ran while one was open for 2% of the time, Pallas kernels for 0%

commit v1 on v0

--- a/solution.py
+++ b/solution.py
@@ -1,3 +1,4 @@
+import functools
 import jax
 import jax.numpy as jnp
 from jax import lax
@@ -5,6 +6,14 @@
 
 RECURRENT_SCALE = 8.0
 EPSILON = 1e-06
+
+
+def _mark_scales(w_in, pos_dim):
+    now = lax.all_gather(w_in, "tp")
+    return jnp.concatenate(now, axis=pos_dim)
+
+
+list_the_frame = functools.partial(_mark_scales, pos_dim=1)
 
 
 def shifted(block, axis, distance):
@@ -109,11 +118,9 @@
 
 def expert_down(active, down_weight):
     columns = down_weight[0]
-    return jnp.dot(
-        lax.all_gather(active, "tp", axis=1, tiled=True),
-        columns,
-        preferred_element_type=jnp.float32,
-    ).astype(jnp.bfloat16)
+    return jnp.dot(list_the_frame(active), columns, preferred_element_type=jnp.float32).astype(
+        jnp.bfloat16
+    )
 
 
 def body(

time: 403 us -> 400 us (level)
  waiting for transfers between devices: 176 us -> 165 us
  local copies, waits for them, and re-layouts: 105 us -> 114 us
    all_gather x1, waiting for transfers between devices: 58.5 us -> 47.6 us  [_mark_scales(): now = lax.all_gather(w_in, 'tp')]
    all_gather x0 -> x1, local copies, waits for them, and re-layouts: none -> 8.64 us  [_mark_scales(): now = lax.all_gather(w_in, 'tp')]
where the time goes in v1:
time: 400 us; the launch traced here: 393 us
  waiting for transfers between devices  165 us (41%)
  local copies, waits for them, and re-layouts  114 us (28%)
  blocking collectives  38.5 us (10%)
  starting transfers between devices  36.2 us (9%)
  matrix products  16.2 us (4%)
  between operations  15.1 us (4%)
  other arithmetic  8.27 us (2%)
    slice x50, local copies, waits for them, and re-layouts, body(): lax.associative_scan(chain_step, (decay, drive), axis=0)  56 us
    all_gather x1, waiting for transfers between devices, _mark_scales(): now = lax.all_gather(w_in, 'tp')  47.6 us
    all_to_all x1, waiting for transfers between devices, sum_at_owner(): lax.all_to_all(pieces, axis, split_axis=0, concat_axis=0, tiled=True)  47.3 us
    all_gather x1, waiting for transfers between devices, piecewise(): blocks = [lax.all_gather(slab, axis) for slab in pieces]  43.7 us
    pad x32, local copies, waits for them, and re-layouts, body(): lax.associative_scan(chain_step, (decay, drive), axis=0)  36.4 us
    all_to_all x1, blocking collectives, body(): lax.all_to_all(outgoing, 'sp', split_axis=0, concat_axis=0, tiled=True)  19.6 us
    all_to_all x1, blocking collectives, body(): lax.all_to_all(result.reshape(tp_size, experts * capacity, -1), 'tp', spl...  18.9 us
    all_to_all x1, waiting for transfers between devices, body(): lax.all_to_all(joined.reshape(experts, capacity, model_width), 'sp', spli...  17.4 us
  transfers between devices with their start and end apart: 6, of which 5 were waited for; matrix products, arithmetic and copies ran while one was open for 2% of the time, Pallas kernels for 0%

profile of v1, /device:TPU:1, one launch (start us, length us, event | category | flops | bytes accessed | tf_op | source)
XLA Modules:
  0.0 392.9 jit_solution(12222472088318258005)
XLA Ops:
  7.4 3.9 collective-permute-start
  18.9 4.5 %slice.371 = f32[256,128]{0,1:T(8,128)S(1)} slice(f32[512,128]{0,1:T(8,128)S(1)} %get-tuple-element.9), slice={[0:511:2], [0:128:1]} | slice | bytes 262144 | tf_op jit(solution)/shard_map/slice | solution.py:171
  23.4 4.5 %slice.372 = f32[256,128]{0,1:T(8,128)S(1)} slice(f32[512,128]{0,1:T(8,128)S(1)} %get-tuple-element.9), slice={[1:512:2], [0:128:1]} | slice | bytes 262144 | tf_op jit(solution)/shard_map/slice | solution.py:171
  27.9 4.5 %slice.370 = f32[256,128]{0,1:T(8,128)S(1)} slice(f32[512,128]{0,1:T(8,128)S(1)} %get-tuple-element.10), slice={[1:512:2], [0:128:1]} | slice | bytes 262144 | tf_op jit(solution)/shard_map/slice | solution.py:171
  32.4 5.0 %slice.374 = f32[256,128]{0,1:T(8,128)S(1)} slice(f32[512,128]{0,1:T(8,128)S(1)} %get-tuple-element.10), slice={[0:511:2], [0:128:1]} | slice | bytes 262144 | tf_op jit(solution)/shard_map/slice | solution.py:171
  67.0 4.5 %slice.369 = f32[255,128]{0,1:T(8,128)S(1)} slice(f32[512,128]{0,1:T(8,128)S(1)} %get-tuple-element.10), slice={[2:512:2], [0:128:1]} | slice | bytes 261120 | tf_op jit(solution)/shard_map/slice | solution.py:171
  71.5 4.9 %slice.434 = f32[255,128]{0,1:T(8,128)S(1)} slice(f32[512,128]{0,1:T(8,128)S(1)} %get-tuple-element.9), slice={[2:512:2], [0:128:1]} | slice | bytes 261120 | tf_op jit(solution)/shard_map/slice | solution.py:171
  94.1 4.5 %pad.145 = f32[512,128]{0,1:T(8,128)S(1)} pad(f32[256,128]{0,1:T(8,128)S(1)} %add.346, f32[]{:T(128)} %constant.25.clone.1), padding=1_0_1x0_0_0 | pad | bytes 393220 | tf_op jit(solution)/shard_map/pad | solution.py:171
  103.3 4.4 %pad.144 = f32[512,128]{0,1:T(8,128)S(1)} pad(f32[256,128]{0,1:T(8,128)S(1)} %pad_maximum_fusion.1, f32[]{:T(128)} %constant.25.clone.1), padding=0_1_1x0_0_0 | pad | bytes 393220 | tf_op jit(solution)/shard_map/pad | solution.py:171
  107.9 4.6 %pad.127 = f32[512,128]{0,1:T(8,128)S(1)} pad(f32[256,128]{0,1:T(8,128)S(1)} %add.336, f32[]{:T(128)} %constant.25.clone.1), padding=1_0_1x0_0_0 | pad | bytes 393220 | tf_op jit(solution)/shard_map/pad | solution.py:171
  112.5 4.4 %pad.126 = f32[512,128]{0,1:T(8,128)S(1)} pad(f32[256,128]{0,1:T(8,128)S(1)} %pad_maximum_fusion, f32[]{:T(128)} %constant.25.clone.1), padding=0_1_1x0_0_0 | pad | bytes 393220 | tf_op jit(solution)/shard_map/pad | solution.py:171
  117.7 12.6 %all-to-all-start = ((f32[32,2,128]{2,1,0:T(2,128)}), f32[32,2,128]{2,1,0:T(2,128)S(1)}, u32[]{:S(2)}, u32[]{:S(2)}) async-start(f32[32,2,128]{2,1,0:T(2,128)} %broadcast_in_dim.64), calls=%async_computation | async-start | bytes 65536 | tf_op jit(solution)/shard_map/all_to_all | solution.py:27
  130.4 8.7 %all-to-all-done = f32[32,2,128]{2,1,0:T(2,128)S(1)} async-done(((f32[32,2,128]{2,1,0:T(2,128)}), f32[32,2,128]{2,1,0:T(2,128)S(1)}, u32[]{:S(2)}, u32[]{:S(2)}) %all-to-all-start) | async-done | bytes 32800 | tf_op jit(solution)/shard_map/all_to_all | solution.py:27
  141.7 9.5 %all-to-all-start.1 = ((bf16[16,32,2048]{2,1,0:T(8,128)(2,1)}), bf16[16,32,2048]{2,1,0:T(8,128)(2,1)S(1)}, u32[]{:S(2)}, u32[]{:S(2)}) async-start(bf16[16,32,2048]{2,1,0:T(8,128)(2,1)} %bitcast.12), calls=%async_computation.1 | async-start | bytes 4194304 | tf_op jit(solution)/shard_map/all_to_all | solution.py:76
  152.9 47.3 %all-to-all-done.1 = bf16[16,32,2048]{2,1,0:T(8,128)(2,1)S(1)} async-done(((bf16[16,32,2048]{2,1,0:T(8,128)(2,1)}), bf16[16,32,2048]{2,1,0:T(8,128)(2,1)S(1)}, u32[]{:S(2)}, u32[]{:S(2)}) %all-to-all-start.1) | async-done | bytes 2097184 | tf_op jit(solution)/shard_map/all_to_all | solution.py:76
  202.2 19.6 %all_to_all.35 = bf16[32,3,2048]{2,1,0:T(4,128)(2,1)S(1)} all-to-all(bf16[32,3,2048]{2,1,0:T(4,128)(2,1)S(1)} %broadcast_select_fusion), channel_id=1, replica_groups=mesh['sp'=32,'tp'=16] {'sp'}, dimensions={0} | all-to-all | bytes 786432 | tf_op jit(solution)/shard_map/all_to_all | solution.py:202
  223.3 43.7 %all-gather.3.cloned.1.call-done = bf16[16,1,96,2048]{3,2,1,0:T(8,128)(2,1)} async-done(((bf16[1,1,96,2048]{3,2,1,0:T(8,128)(2,1)}), bf16[16,1,96,2048]{3,2,1,0:T(8,128)(2,1)}) %all-gather.3.cloned.1.call-update) | async-done | bytes 6291472 | tf_op jit(solution)/shard_map/all_gather | solution.py:90
  266.9 4.7 %fusion.2 = f32[16,96,128]{2,1,0:T(8,128)S(1)} fusion(bf16[16,1,96,2048]{3,2,1,0:T(8,128)(2,1)} %all-gather.3.cloned.1.call-done, bf16[1,2048,128]{2,1,0:T(8,128)(2,1)S(1)} %copy-done.5), kind=kOutput, calls=%fused_computation.4 | convolution fusion | flops 805306368 | bytes 7602176 | tf_op jit(solution)/shard_map/vmap()/dot_general | solution.py:114
  274.3 47.6 %all-gather.5.cloned.1.call-done = bf16[16,1536,128]{2,1,0:T(8,128)(2,1)} async-done(((bf16[1,1536,128]{2,1,0:T(8,128)(2,1)}), bf16[16,1536,128]{2,1,0:T(8,128)(2,1)}) %all-gather.5.cloned.1.call-update) | async-done | bytes 6291472 | tf_op jit(solution)/shard_map/all_gather | solution.py:12
  321.9 8.6 %copy.107 = bf16[16,1536,128]{1,2,0:T(8,128)(2,1)} copy(bf16[16,1536,128]{2,1,0:T(8,128)(2,1)} %all-gather.5.cloned.1.call-done) | data formatting | bytes 12582912 | tf_op jit(solution)/shard_map/all_gather | solution.py:12
  330.6 4.6 %convolution_convert_fusion.1 = bf16[1536,128]{1,0:T(8,128)(2,1)S(1)} fusion(bf16[1536,2048]{0,1:T(8,128)(2,1)} %bitcast.88, bf16[1,2048,128]{2,1,0:T(8,128)(2,1)S(1)} %copy-done.7), kind=kOutput, calls=%fused_computation.8 | convolution fusion | flops 805502976 | bytes 7208960 | tf_op jit(solution)/shard_map/dot_general | solution.py:121
  335.2 18.9 %all_to_all.36 = bf16[16,96,128]{2,1,0:T(8,128)(2,1)S(1)} all-to-all(bf16[16,96,128]{2,1,0:T(8,128)(2,1)S(1)} %bitcast.101), channel_id=1, replica_groups=mesh['sp'=32,'tp'=16] {'tp'}, dimensions={0} | all-to-all | bytes 786432 | tf_op jit(solution)/shard_map/all_to_all | solution.py:214
  355.2 9.9 %all-to-all-start.4 = ((bf16[32,3,2048]{2,1,0:T(4,128)(2,1)}), bf16[32,3,2048]{2,1,0:T(4,128)(2,1)S(1)}, u32[]{:S(2)}, u32[]{:S(2)}) async-start(bf16[32,3,2048]{2,1,0:T(4,128)(2,1)} %reshape.156), calls=%async_computation.4 | async-start | bytes 1048576 | tf_op jit(solution)/shard_map/all_to_all | solution.py:221
  365.4 17.4 %all-to-all-done.4 = bf16[32,3,2048]{2,1,0:T(4,128)(2,1)S(1)} async-done(((bf16[32,3,2048]{2,1,0:T(4,128)(2,1)}), bf16[32,3,2048]{2,1,0:T(4,128)(2,1)S(1)}, u32[]{:S(2)}, u32[]{:S(2)}) %all-to-all-start.4) | async-done | bytes 393248 | tf_op jit(solution)/shard_map/all_to_all | solution.py:221
  (232 shorter events, 75.2 us)
Async XLA Ops:
  6.5 133.0 %copy-start = (bf16[128,2048]{1,0:T(8,128)(2,1)S(1)}, bf16[128,2048]{1,0:T(8,128)(2,1)}, u32[]{:S(2)}) copy-start(bf16[128,2048]{1,0:T(8,128)(2,1)} %param.23) | copy-start | bytes 1572868
  7.4 8.6 %collective-permute-start = (bf16[3,128]{0,1:T(8,128)(2,1)S(1)}, bf16[3,128]{0,1:T(8,128)(2,1)S(1)}, u32[]{:S(2)}, u32[]{:S(2)}) collective-permute-start(bf16[3,128]{0,1:T(8,128)(2,1)S(1)} %copy.86), channel_id=1, source_target_pairs={{0,16},{16,32},{32,48},{48,64},{64,80},{80,96},{96,112},{112,128},... | collective-permute-start | bytes 2312 | tf_op jit(solution)/shard_map/ppermute | solution.py:22
  107.8 92.8 %copy-start.1 = (bf16[32,2048]{1,0:T(8,128)(2,1)S(1)}, bf16[32,2048]{1,0:T(8,128)(2,1)}, u32[]{:S(2)}) copy-start(bf16[32,2048]{1,0:T(8,128)(2,1)} %param.15) | copy-start | bytes 393220
  112.4 88.3 %copy-start.2 = (f32[2048]{0:T(1024)S(1)}, f32[2048]{0:T(1024)}, u32[]{:S(2)}) copy-start(f32[2048]{0:T(1024)} %param.24) | copy-start | bytes 24580
  117.7 21.3 %all-to-all-start = ((f32[32,2,128]{2,1,0:T(2,128)}), f32[32,2,128]{2,1,0:T(2,128)S(1)}, u32[]{:S(2)}, u32[]{:S(2)}) async-start(f32[32,2,128]{2,1,0:T(2,128)} %broadcast_in_dim.64), calls=%async_computation | async-start | bytes 65536 | tf_op jit(solution)/shard_map/all_to_all | solution.py:27
  141.7 58.5 %all-to-all-start.1 = ((bf16[16,32,2048]{2,1,0:T(8,128)(2,1)}), bf16[16,32,2048]{2,1,0:T(8,128)(2,1)S(1)}, u32[]{:S(2)}, u32[]{:S(2)}) async-start(bf16[16,32,2048]{2,1,0:T(8,128)(2,1)} %bitcast.12), calls=%async_computation.1 | async-start | bytes 4194304 | tf_op jit(solution)/shard_map/all_to_all | solution.py:76
  151.2 115.8 %copy-start.5 = (bf16[1,2048,128]{2,1,0:T(8,128)(2,1)S(1)}, bf16[1,2048,128]{2,1,0:T(8,128)(2,1)}, u32[]{:S(2)}) copy-start(bf16[1,2048,128]{2,1,0:T(8,128)(2,1)} %param.27) | copy-start | bytes 1572868
  151.2 115.8 %all-gather.3.cloned.1.call-start = ((), (), s32[]{:S(2)}) async-start(), calls=%async_computation.5 | async-start | bytes 6684672 | tf_op jit(solution)/shard_map/all_gather | solution.py:90
  222.9 48.7 %copy-start.6 = (bf16[1,2048,128]{2,1,0:T(8,128)(2,1)S(1)}, bf16[1,2048,128]{2,1,0:T(8,128)(2,1)}, u32[]{:S(2)}) copy-start(bf16[1,2048,128]{2,1,0:T(8,128)(2,1)} %param.28) | copy-start | bytes 1572868
  223.0 99.0 %all-gather.5.cloned.1.call-start = ((), (), s32[]{:S(2)}) async-start(), calls=%async_computation.6 | async-start | bytes 6684672 | tf_op jit(solution)/shard_map/all_gather | solution.py:12
  266.9 4.8 %copy-start.4 = (bf16[16,1,96,2048]{3,2,1,0:T(8,128)(2,1)S(1)}, bf16[16,1,96,2048]{3,2,1,0:T(8,128)(2,1)}, u32[]{:S(2)}) copy-start(bf16[16,1,96,2048]{3,2,1,0:T(8,128)(2,1)} %all-gather.3.cloned.1.call-done) | copy-start | bytes 18874372
  274.3 56.3 %copy-start.7 = (bf16[1,2048,128]{2,1,0:T(8,128)(2,1)S(1)}, bf16[1,2048,128]{2,1,0:T(8,128)(2,1)}, u32[]{:S(2)}) copy-start(bf16[1,2048,128]{2,1,0:T(8,128)(2,1)} %param.29) | copy-start | bytes 1572868
  330.6 34.7 %copy-start.3 = (f32[32,2]{0,1:T(2,128)S(1)}, f32[32,2]{0,1:T(2,128)}, u32[]{:S(2)}) copy-start(f32[32,2]{0,1:T(2,128)} %param.26) | copy-start | bytes 772
  355.2 27.6 %all-to-all-start.4 = ((bf16[32,3,2048]{2,1,0:T(4,128)(2,1)}), bf16[32,3,2048]{2,1,0:T(4,128)(2,1)S(1)}, u32[]{:S(2)}, u32[]{:S(2)}) async-start(bf16[32,3,2048]{2,1,0:T(4,128)(2,1)} %reshape.156), calls=%async_computation.4 | async-start | bytes 1048576 | tf_op jit(solution)/shard_map/all_to_all | solution.py:221
Sparse Core Ops, SparseCore 0:
  223.1 43.8 all-gather.2
  274.4 47.4 all-gather.4
